TPU v7x, 512 devices: a whole 4x8x8 slice. The times are simulated.
512 devices in a mesh: sp: 128 (over z, y, core), tp: 4 (over x).
Axes of the slice: x: 4, y: 8, z: 8, core: 2. Of those that a mesh axis runs over, the one named last changes fastest.
Arguments:
- tokens: bfloat16 [65536, 2048], P('sp'), may hold values from -6 to 6
- norm_gain: bfloat16 [2048], replicated, may hold values from 0.099609375 to 1.8984375
- w_conv_value: bfloat16 [2048, 2048], P('sp', 'tp'), may hold values from -0.125 to 0.125
- w_conv_gate: bfloat16 [2048, 2048], P('sp', 'tp'), may hold values from -0.125 to 0.125
- w_query: bfloat16 [2048, 2048], P('sp', 'tp'), may hold values from -0.125 to 0.125
- w_key: bfloat16 [2048, 512], P('sp', 'tp'), may hold values from -0.125 to 0.125
- w_value: bfloat16 [2048, 512], P('sp', 'tp'), may hold values from -0.125 to 0.125
- conv_taps: float32 [31, 2048], P(None, 'tp'), as said below
- ln_gain: float32 [2048], P('tp'), may hold values from 0.1 to 1.9
- sinks: float32 [32], P('tp'), may hold values from 3 to 6
- out_conv: bfloat16 [2048, 2048], P('tp', 'sp'), may hold values from -0.125 to 0.125
- out_attn: bfloat16 [2048, 2048], P('tp', 'sp'), may hold values from -0.5 to 0.5
Outputs:
- mixed: bfloat16 [65536, 2048], P(('sp', 'tp'))
- log_sums: float32 [32, 65536], P('tp', 'sp')
Inputs may be any that keep to these rules, and one draw needn't show every extreme that they name: `conv_taps`: each tap lies within 30 / sqrt(31) in magnitude.
All inputs are finite; a program needn't handle non-finite values.
Results may differ from a plain program's by a relative error of at most 0.017.
Values may be sent and summed in bfloat16 or wider, within the bound.
A program may use at most 64 MiB of HBM per device.

v0:
```python
import jax
import jax.numpy as jnp
from jax import lax
from jax.sharding import PartitionSpec as P

CONV_CH = 2048
HEADS = 32
KV_HEADS = 8
HEAD_DIM = 64
WINDOW = 128
NORM_EPS = 1e-06
CHANNEL_EPS = 1e-05
ROPE_BASE = 10000.0


def sent_together(arrays, axis, dim, along):
    widths = [a.shape[along] for a in arrays]
    both = jnp.concatenate(arrays, axis=along)
    whole = lax.all_gather(both, axis, axis=dim, tiled=True)
    return tuple(jnp.split(whole, [sum(widths[:k]) for k in range(1, len(widths))], axis=along))


def shifted(value, axis, steps):
    count = lax.axis_size(axis)
    initial, last = (max(0, -steps), min(count, count - steps))
    return lax.ppermute(value, axis, [(source, source + steps) for source in range(initial, last)])


def from_everyone(shard, axis):
    peers = lax.axis_size(axis)
    return lax.all_to_all(
        jnp.broadcast_to(shard[None], (peers, *shard.shape)), axis, 0, 0, tiled=True
    )


def taken_together(shard, axis):
    everything = from_everyone(shard, axis)
    return jnp.sum(everything, axis=0)


def packed_total(arrays, axis):
    ravelled, at, finished = (jnp.concatenate([a.reshape(-1) for a in arrays]), 0, [])
    subtotal = taken_together(ravelled, axis)
    for a in arrays:
        finished.append(subtotal[at : at + a.size].reshape(a.shape))
        at += a.size
    return tuple(finished)


def turned_gather(arrays, axis, dims):
    turned = [jnp.moveaxis(a, dim, 0) for a, dim in zip(arrays, dims)]
    both = jnp.concatenate([t.reshape(len(t), -1) for t in turned], axis=1)
    whole, at, finished = (lax.all_gather(both, axis, axis=0, tiled=True), 0, [])
    for t, dim in zip(turned, dims):
        piece = whole[:, at : at + t[0].size].reshape(-1, *t.shape[1:])
        finished.append(jnp.moveaxis(piece, 0, dim))
        at += t[0].size
    return tuple(finished)


def cut_along(shard, dim, peers):
    dims = shard.shape
    pieces = shard.reshape(*dims[:dim], peers, dims[dim] // peers, *dims[dim + 1 :])
    return jnp.moveaxis(pieces, dim, 0)


def summed_on_arrival(shard, axis, dim):
    pieces = cut_along(shard, dim, lax.axis_size(axis))
    arrived = lax.all_to_all(pieces, axis, split_axis=0, concat_axis=0, tiled=True)
    return arrived.astype(jnp.float32).sum(axis=0)


def rotate(heads, positions):
    half_dim = heads.shape[-1] // 2
    inverse = ROPE_BASE ** (-jnp.arange(half_dim, dtype=jnp.float32) / half_dim)
    angles = positions.astype(jnp.float32)[:, None] * inverse[None, :]
    cosine = jnp.cos(angles)[:, None, :]
    sine = jnp.sin(angles)[:, None, :]
    as_float = heads.astype(jnp.float32)
    front_part = as_float[..., :half_dim]
    back_part = as_float[..., half_dim:]
    return jnp.concatenate(
        [front_part * cosine - back_part * sine, back_part * cosine + front_part * sine], axis=-1
    )


def shards(
    tokens,
    norm_gain,
    w_conv_value,
    w_conv_gate,
    w_query,
    w_key,
    w_value,
    conv_taps,
    ln_gain,
    sinks,
    out_conv,
    out_attn,
):
    as_float = tokens.astype(jnp.float32)
    normed = (
        as_float
        * lax.rsqrt(jnp.mean(as_float * as_float, axis=-1, keepdims=True) + NORM_EPS)
        * norm_gain.astype(jnp.float32)
    ).astype(jnp.bfloat16)
    row_count = normed.shape[0]
    pieces = sent_together((w_conv_value, w_conv_gate, w_query, w_key, w_value), "sp", 0, 1)
    projected = tuple(
        (jnp.dot(normed, piece, preferred_element_type=jnp.float32) for piece in pieces)
    )
    conv_value, conv_gate, query_raw, key_raw, value_rows = [
        item.astype(jnp.bfloat16) for item in projected
    ]
    glu = (conv_value.astype(jnp.float32) * jax.nn.sigmoid(conv_gate.astype(jnp.float32))).astype(
        jnp.bfloat16
    )
    offset = lax.axis_index("sp") * row_count
    positions = offset + jnp.arange(row_count, dtype=jnp.int32)
    query_heads = query_raw.shape[1] // HEAD_DIM
    key_heads = key_raw.shape[1] // HEAD_DIM
    query = rotate(query_raw.reshape(row_count, query_heads, HEAD_DIM), positions).astype(
        jnp.bfloat16
    )
    key = rotate(key_raw.reshape(row_count, key_heads, HEAD_DIM), positions).astype(jnp.bfloat16)
    reach = conv_taps.shape[0] - 1
    key_tail = key[row_count - WINDOW :]
    value_tail = value_rows.reshape(row_count, key_heads, HEAD_DIM)[row_count - WINDOW :]
    glu_tail = glu[row_count - reach :]
    glu_before = shifted(glu_tail, "sp", 1)
    key_before, value_before = shifted((key_tail, value_tail), "sp", 1)
    extended = jnp.concatenate([glu_before, glu], axis=0).astype(jnp.float32)
    conv_out = jnp.zeros((row_count, glu.shape[1]), jnp.float32)
    for tap in range(reach + 1):
        conv_out = conv_out + conv_taps[tap][None, :] * extended[tap : tap + row_count]
    sum_first = jnp.sum(conv_out, axis=-1)
    sum_second = jnp.sum(conv_out * conv_out, axis=-1)
    total_first, total_second = packed_total((sum_first, sum_second), "tp")
    mean = (total_first / CONV_CH)[:, None]
    var = (total_second / CONV_CH)[:, None] - mean * mean
    conv_branch = jax.nn.silu(
        (conv_out - mean) * lax.rsqrt(var + CHANNEL_EPS) * ln_gain[None, :]
    ).astype(jnp.bfloat16)
    group = HEADS // KV_HEADS
    blocks = row_count // WINDOW
    q_blocks = query.reshape(blocks, WINDOW, key_heads, group, HEAD_DIM)
    key_blocks = jnp.concatenate([key_before, key], axis=0).reshape(
        blocks + 1, WINDOW, key_heads, HEAD_DIM
    )
    value_all = jnp.concatenate(
        [value_before, value_rows.reshape(row_count, key_heads, HEAD_DIM)], axis=0
    )
    value_blocks = value_all.reshape(blocks + 1, WINDOW, key_heads, HEAD_DIM)
    key_window = jnp.concatenate([key_blocks[:-1], key_blocks[1:]], axis=1)
    value_window = jnp.concatenate([value_blocks[:-1], value_blocks[1:]], axis=1)
    scores = jnp.einsum(
        "nqhgd,nkhd->nhgqk", q_blocks, key_window, preferred_element_type=jnp.float32
    ) * HEAD_DIM ** (-0.5)
    query_index = jnp.arange(WINDOW)[:, None] + WINDOW
    key_index = jnp.arange(2 * WINDOW)[None, :]
    band = (key_index <= query_index) & (query_index - key_index < WINDOW)
    block_index = jnp.arange(blocks)[:, None, None]
    allowed = band[None] & (offset + block_index * WINDOW + key_index[None] - WINDOW >= 0)
    allowed = allowed[:, None, None]
    totals = jnp.sum(jnp.where(allowed, jnp.exp(scores), 0.0), axis=-1)
    totals = totals + jnp.exp(sinks).reshape(1, key_heads, group, 1)
    log_total = jnp.log(totals)
    weights = jnp.where(allowed, jnp.exp(scores - log_total[..., None]), 0.0).astype(jnp.bfloat16)
    attended = jnp.einsum(
        "nhgqk,nkhd->nqhgd", weights, value_window, preferred_element_type=jnp.float32
    )
    attn_branch = attended.astype(jnp.bfloat16).reshape(row_count, query_heads * HEAD_DIM)
    log_sums = log_total.transpose(1, 2, 0, 3).reshape(query_heads, row_count)
    cols_conv, cols_attn = turned_gather((out_conv, out_attn), "sp", (1, 1))
    mixed = summed_on_arrival(
        (
            jnp.dot(conv_branch, cols_conv, preferred_element_type=jnp.float32)
            + jnp.dot(attn_branch, cols_attn, preferred_element_type=jnp.float32)
        ).astype(jnp.bfloat16),
        "tp",
        0,
    )
    return (mixed.astype(jnp.bfloat16), log_sums)


def solution(mesh):
    in_specs = (
        P("sp", None),
        P(),
        P("sp", "tp"),
        P("sp", "tp"),
        P("sp", "tp"),
        P("sp", "tp"),
        P("sp", "tp"),
        P(None, "tp"),
        P("tp"),
        P("tp"),
        P("tp", "sp"),
        P("tp", "sp"),
    )
    out_specs = (P(("sp", "tp"), None), P("tp", "sp"))
    return jax.shard_map(shards, mesh=mesh, in_specs=in_specs, out_specs=out_specs, check_vma=False)
```

profile of v0, /device:TPU:1, one launch (start us, length us, event | category | flops | bytes accessed | tf_op | source)
XLA Modules:
  0.0 231.2 jit_solution(13513248119261540660)
XLA Ops:
  7.2 0.9 constant_dynamic-update-slice_fusion.4
  8.1 0.7 constant_dynamic-update-slice_fusion.3
  8.8 0.7 constant_dynamic-update-slice_fusion.2
  9.5 0.7 constant_dynamic-update-slice_fusion.1
  10.2 0.7 constant_dynamic-update-slice_fusion
  10.9 0.6 copy-done.2
  11.6 1.3 pad_maximum_fusion.4
  13.0 0.7 convert_element_type.78
  13.7 0.7 exp.19
  15.1 2.1 fusion
  17.2 1.0 fusion.126
  18.2 1.7 fusion.125
  20.5 84.2 %all-gather.3.cloned.1.call-done = bf16[2048,1792]{1,0:T(8,128)(2,1)} async-done(((bf16[16,1792]{1,0:T(8,128)(2,1)}), bf16[2048,1792]{1,0:T(8,128)(2,1)}) %all-gather.3.cloned.1.call-update) | async-done | bytes 7340048 | tf_op jit(solution)/shard_map/all_gather | solution.py:19
  104.7 2.6 %convolution_convert_fusion.1 = bf16[512,128]{0,1:T(8,128)(2,1)S(1)} fusion(bf16[2048,1792]{1,0:T(8,128)(2,1)} %all-gather.3.cloned.1.call-done, bf16[512,2048]{1,0:T(8,128)(2,1)} %param.12, f32[2048]{0:T(1024)S(1)} %convert_element_type.78, f32[512]{0:T(512)S(1)} %add_rsqrt_fusion.1), kind=kOutput, calls=%fused_computation.41 | convolution fusion | flops 272695296 | bytes 2762752 | tf_op jit(solution)/shard_map/dot_general | solution.py:110
  107.4 2.1 convolution_convert_fusion
  109.6 3.0 %collective-permute-start.2 = (bf16[128,2,64]{0,2,1:T(8,128)(2,1)S(1)}, bf16[128,2,64]{0,2,1:T(8,128)(2,1)S(1)}, u32[]{:S(2)}, u32[]{:S(2)}) collective-permute-start(bf16[128,2,64]{0,2,1:T(8,128)(2,1)S(1)} %pad_maximum_fusion.3), channel_id=1, source_target_pairs={{0,4},{4,8},{8,12},{12,16},{16,20},{20,24},{24,28},{28,32},{32,36}... | collective-permute-start | bytes 98312 | tf_op jit(solution)/shard_map/ppermute | solution.py:26
  112.6 3.0 %fusion.47 = bf16[512,512]{0,1:T(8,128)(2,1)S(1)} fusion(bf16[2048,1792]{1,0:T(8,128)(2,1)} %all-gather.3.cloned.1.call-done, bf16[512,2048]{1,0:T(8,128)(2,1)S(1)} %copy-done, f32[2048]{0:T(1024)S(1)} %convert_element_type.78, f32[512]{0:T(512)S(1)} %add_rsqrt_fusion.1), kind=kOutput, calls=%fused_computation.35 | convolution fusion | flops 1078198272 | bytes 4728832 | tf_op jit(solution)/shard_map/dot_general | solution.py:110
  115.7 1.5 fusion.56
  117.2 1.3 fusion.50
  118.5 2.1 collective-permute-start
  121.1 3.7 %collective-permute-start.1 = (bf16[128,2,64]{0,2,1:T(8,128)(2,1)S(1)}, bf16[128,2,64]{0,2,1:T(8,128)(2,1)S(1)}, u32[]{:S(2)}, u32[]{:S(2)}) collective-permute-start(bf16[128,2,64]{0,2,1:T(8,128)(2,1)S(1)} %bitcast.113), channel_id=1, source_target_pairs={{0,4},{4,8},{8,12},{12,16},{16,20},{20,24},{24,28},{28,32},{32,36}... | collective-permute-start | bytes 98312 | tf_op jit(solution)/shard_map/ppermute | solution.py:26
  125.1 5.1 %fusion.123 = (f32[512]{0:T(512)S(1)}, f32[512]{0:T(512)S(1)}, f32[512,512]{1,0:T(8,128)S(1)}) fusion(f32[542,512]{1,0:T(8,128)S(1)} %maximum_convert_fusion, f32[512]{0:T(512)S(1)} %bitcast.127, f32[512]{0:T(512)S(1)} %bitcast.128, f32[512]{0:T(512)S(1)} %bitcast.130, f32[512]{0:T(512)S(1)} %bitcast.131, f32[512]{0:T(512)S(1)} %bitcast.132, ...), kind=kLoop, calls=%fused_computation.167 | loop fusion | flops 16776192 | bytes 33622016 | tf_op jit(solution)/shard_map/reduce_sum | solution.py:136
  130.2 0.6 broadcast_in_dim.14
  130.8 4.0 %all-to-all-start = ((f32[4,1,1024]{2,1,0:T(1,128)}), f32[4,1,1024]{2,1,0:T(1,128)S(1)}, u32[]{:S(2)}, u32[]{:S(2)}) async-start(f32[4,1,1024]{2,1,0:T(1,128)} %broadcast_in_dim.14), calls=%async_computation | async-start | bytes 32768 | tf_op jit(solution)/shard_map/all_to_all | solution.py:31
  134.8 1.1 fusion.4
  136.1 0.9 fusion.59
  137.4 1.6 all-to-all-done
  139.0 49.8 %all-gather.5.cloned.1.call-done = bf16[2048,1024]{1,0:T(8,128)(2,1)} async-done(((bf16[16,1024]{1,0:T(8,128)(2,1)}), bf16[2048,1024]{1,0:T(8,128)(2,1)}) %all-gather.5.cloned.1.call-update) | async-done | bytes 4194320 | tf_op jit(solution)/shard_map/all_gather | solution.py:53
  188.9 3.2 %fusion.13 = f32[512,2048]{1,0:T(8,128)S(1)} fusion(bf16[2048,1024]{1,0:T(8,128)(2,1)} %all-gather.5.cloned.1.call-done, f32[512,512]{1,0:T(8,128)S(1)} %get-tuple-element.4, f32[512]{0:T(512)S(1)} %copy-done.8, f32[512]{0:T(512)S(1)} %get-tuple-element.41, f32[512]{0:T(512)S(1)} %get-tuple-element.40), kind=kOutput, calls=%fused_computation.17 | convolution fusion | flops 1075838976 | bytes 7346176 | tf_op jit(solution)/shard_map/dot_general | solution.py:177
  192.1 1.3 add_convert_fusion
  193.4 29.6 %all_to_all.11 = bf16[4,128,2048]{2,1,0:T(8,128)(2,1)S(1)} all-to-all(bf16[4,128,2048]{2,1,0:T(8,128)(2,1)S(1)} %bitcast.108), channel_id=1, replica_groups=mesh['sp'=128,'tp'=4] {'tp'}, dimensions={0} | all-to-all | bytes 4194304 | tf_op jit(solution)/shard_map/all_to_all | solution.py:69
  223.0 1.3 reduce_sum.62
  (61 shorter events, 2.8 us)
Async XLA Ops:
  7.2 100.2 %copy-start = (bf16[512,2048]{1,0:T(8,128)(2,1)S(1)}, bf16[512,2048]{1,0:T(8,128)(2,1)}, u32[]{:S(2)}) copy-start(bf16[512,2048]{1,0:T(8,128)(2,1)} %param.12) | copy-start | bytes 6291460
  7.2 97.5 %all-gather.3.cloned.1.call-start = ((), (), s32[]{:S(2)}) async-start(), calls=%async_computation.2 | async-start | bytes 7397376 | tf_op jit(solution)/shard_map/all_gather | solution.py:19
  10.9 0.6 copy-start.2
  11.6 177.3 %all-gather.5.cloned.1.call-start = ((), (), s32[]{:S(2)}) async-start(), calls=%async_computation.3 | async-start | bytes 4227072 | tf_op jit(solution)/shard_map/all_gather | solution.py:53
  107.3 8.3 %slice-start = ((s8[7340032]{0:T(1024)(128)(4,1)}), s8[4194304]{0:T(1024)(128)(4,1)S(1)}, s32[]{:S(2)}) async-start(s8[7340032]{0:T(1024)(128)(4,1)} %bitcast.148), calls=%async_computation.4 | async-start | bytes 8388608
  109.5 6.1 %slice-start.1 = ((s8[7340032]{0:T(1024)(128)(4,1)}), s8[3145728]{0:T(1024)(128)(4,1)S(1)}, s32[]{:S(2)}) async-start(s8[7340032]{0:T(1024)(128)(4,1)} %bitcast.148), calls=%async_computation.5 | async-start | bytes 6291456
  109.6 25.2 %collective-permute-start.2 = (bf16[128,2,64]{0,2,1:T(8,128)(2,1)S(1)}, bf16[128,2,64]{0,2,1:T(8,128)(2,1)S(1)}, u32[]{:S(2)}, u32[]{:S(2)}) collective-permute-start(bf16[128,2,64]{0,2,1:T(8,128)(2,1)S(1)} %pad_maximum_fusion.3), channel_id=1, source_target_pairs={{0,4},{4,8},{8,12},{12,16},{16,20},{20,24},{24,28},{28,32},{32,36}... | collective-permute-start | bytes 98312 | tf_op jit(solution)/shard_map/ppermute | solution.py:26
  118.5 6.6 %copy-start.4 = (f32[1,512]{1,0:T(1,128)S(1)}, f32[1,512]{1,0:T(1,128)}, u32[]{:S(2)}) copy-start(f32[1,512]{1,0:T(1,128)} %get-tuple-element.25) | copy-start | bytes 6148
  118.5 6.6 %copy-start.5 = (f32[1,512]{1,0:T(1,128)S(1)}, f32[1,512]{1,0:T(1,128)}, u32[]{:S(2)}) copy-start(f32[1,512]{1,0:T(1,128)} %get-tuple-element.26) | copy-start | bytes 6148
  118.5 6.6 %copy-start.6 = (f32[1,512]{1,0:T(1,128)S(1)}, f32[1,512]{1,0:T(1,128)}, u32[]{:S(2)}) copy-start(f32[1,512]{1,0:T(1,128)} %get-tuple-element.27) | copy-start | bytes 6148
  118.5 6.3 %collective-permute-start = (bf16[30,512]{1,0:T(8,128)(2,1)S(1)}, bf16[30,512]{1,0:T(8,128)(2,1)S(1)}, u32[]{:S(2)}, u32[]{:S(2)}) collective-permute-start(bf16[30,512]{1,0:T(8,128)(2,1)S(1)} %slice.319), channel_id=1, source_target_pairs={{0,4},{4,8},{8,12},{12,16},{16,20},{20,24},{24,28},{28,32},{32,36}... | collective-permute-start | bytes 92168 | tf_op jit(solution)/shard_map/ppermute | solution.py:26
  121.1 13.7 %collective-permute-start.1 = (bf16[128,2,64]{0,2,1:T(8,128)(2,1)S(1)}, bf16[128,2,64]{0,2,1:T(8,128)(2,1)S(1)}, u32[]{:S(2)}, u32[]{:S(2)}) collective-permute-start(bf16[128,2,64]{0,2,1:T(8,128)(2,1)S(1)} %bitcast.113), channel_id=1, source_target_pairs={{0,4},{4,8},{8,12},{12,16},{16,20},{20,24},{24,28},{28,32},{32,36}... | collective-permute-start | bytes 98312 | tf_op jit(solution)/shard_map/ppermute | solution.py:26
  130.2 5.8 %copy-start.7 = (f32[2,4]{1,0:T(2,128)S(1)}, f32[2,4]{1,0:T(2,128)}, u32[]{:S(2)}) copy-start(f32[2,4]{1,0:T(2,128)} %add.243) | copy-start | bytes 100
  130.8 8.2 %all-to-all-start = ((f32[4,1,1024]{2,1,0:T(1,128)}), f32[4,1,1024]{2,1,0:T(1,128)S(1)}, u32[]{:S(2)}, u32[]{:S(2)}) async-start(f32[4,1,1024]{2,1,0:T(1,128)} %broadcast_in_dim.14), calls=%async_computation | async-start | bytes 32768 | tf_op jit(solution)/shard_map/all_to_all | solution.py:31
  135.9 52.9 %copy-start.8 = (f32[512]{0:T(512)S(1)}, f32[512]{0:T(512)}, u32[]{:S(2)}) copy-start(f32[512]{0:T(512)} %param.20) | copy-start | bytes 6148
  136.1 56.0 %copy-start.3 = (f32[4,2,4,128]{3,2,1,0:T(4,128)}, f32[4,2,4,128]{3,2,1,0:T(4,128)S(1)}, u32[]{:S(2)}) copy-start(f32[4,2,4,128]{3,2,1,0:T(4,128)S(1)} %add_log_fusion) | copy-start | bytes 49156
  188.9 3.2 %copy-start.1 = (bf16[2048,1024]{1,0:T(8,128)(2,1)S(1)}, bf16[2048,1024]{1,0:T(8,128)(2,1)}, u32[]{:S(2)}) copy-start(bf16[2048,1024]{1,0:T(8,128)(2,1)} %all-gather.5.cloned.1.call-done) | copy-start | bytes 12582916
Sparse Core Ops, SparseCore 0:
  11.7 92.9 all-gather.2
  107.8 80.9 all-gather.4
where the time goes:
time: 232 us; the launch traced here: 231 us
  waiting for transfers between devices  136 us (59%)
  blocking collectives  29.6 us (13%)
  matrix products  16.9 us (7%)
  between operations  14.5 us (6%)
  starting transfers between devices  12.9 us (6%)
  other arithmetic  11.8 us (5%)
  local copies, waits for them, and re-layouts  9.71 us (4%)
    all_gather x1, waiting for transfers between devices, sent_together(): whole = lax.all_gather(both, axis, axis=dim, tiled=True)  84.2 us
    all_gather x1, waiting for transfers between devices, turned_gather(): lax.all_gather(both, axis, axis=0, tiled=True)  49.8 us
    all_to_all x1, blocking collectives, summed_on_arrival(): lax.all_to_all(pieces, axis, split_axis=0, concat_axis=0, tiled=True)  29.6 us
    dot_general x5, matrix products, shards(): jnp.dot(normed, piece, preferred_element_type=jnp.float32)  10.4 us
    ppermute x3, starting transfers between devices, shifted(): lax.ppermute(value, axis, [(source, source + steps) for source in range(i...  8.87 us
    reduce_sum x1, other arithmetic, shards(): sum_first = jnp.sum(conv_out, axis=-1)  5.05 us
  transfers between devices with their start and end apart: 6, of which 3 were waited for; matrix products, arithmetic and copies ran while one was open for 12% of the time, Pallas kernels for 0%

commit v1 on v0

--- a/solution.py
+++ b/solution.py
@@ -13,6 +13,13 @@
 ROPE_BASE = 10000.0
 
 
+def exchange_gather(x, mesh_axis, dim):
+    size = lax.axis_size(mesh_axis)
+    parts = jnp.stack([x for _ in range(size)])
+    parts = lax.all_to_all(parts, mesh_axis, split_axis=0, concat_axis=0)
+    return jnp.concatenate(parts, axis=dim)
+
+
 def sent_together(arrays, axis, dim, along):
     widths = [a.shape[along] for a in arrays]
     both = jnp.concatenate(arrays, axis=along)
@@ -50,7 +57,7 @@
 def turned_gather(arrays, axis, dims):
     turned = [jnp.moveaxis(a, dim, 0) for a, dim in zip(arrays, dims)]
     both = jnp.concatenate([t.reshape(len(t), -1) for t in turned], axis=1)
-    whole, at, finished = (lax.all_gather(both, axis, axis=0, tiled=True), 0, [])
+    whole, at, finished = (exchange_gather(both, axis, 0), 0, [])
     for t, dim in zip(turned, dims):
         piece = whole[:, at : at + t[0].size].reshape(-1, *t.shape[1:])
         finished.append(jnp.moveaxis(piece, 0, dim))

time: 232 us -> 291 us (1.25)
  the two profiles are of different devices: /device:TPU:1 before, /device:TPU:32 now
where the time goes in v1:
time: 291 us; the launch traced here: 290 us
  waiting for transfers between devices  174 us (60%)
  blocking collectives  29.1 us (10%)
  starting transfers between devices  22.6 us (8%)
  matrix products  22.3 us (8%)
  between operations  14.4 us (5%)
  other arithmetic  14.1 us (5%)
  local copies, waits for them, and re-layouts  13.4 us (5%)
    all_gather x1, waiting for transfers between devices, sent_together(): whole = lax.all_gather(both, axis, axis=dim, tiled=True)  86.2 us
    ppermute x3, waiting for transfers between devices, shifted(): lax.ppermute(value, axis, [(source, source + steps) for source in range(i...  75.7 us
    all_to_all x1, blocking collectives, summed_on_arrival(): lax.all_to_all(pieces, axis, split_axis=0, concat_axis=0, tiled=True)  29.1 us
    dot_general x5, matrix products, shards(): jnp.dot(normed, piece, preferred_element_type=jnp.float32)  13.4 us
    all_to_all x1, starting transfers between devices, exchange_gather(): parts = lax.all_to_all(parts, mesh_axis, split_axis=0, concat_axis=0)  11.5 us
    ppermute x3, starting transfers between devices, shifted(): lax.ppermute(value, axis, [(source, source + steps) for source in range(i...  6.81 us
    all_to_all x1, waiting for transfers between devices, exchange_gather(): parts = lax.all_to_all(parts, mesh_axis, split_axis=0, concat_axis=0)  6.62 us
  transfers between devices with their start and end apart: 6, of which 5 were waited for; matrix products, arithmetic and copies ran while one was open for 8% of the time, Pallas kernels for 0%

profile of v1, /device:TPU:32, one launch (start us, length us, event | category | flops | bytes accessed | tf_op | source)
XLA Modules:
  0.0 289.7 jit_solution(15958793626473537208)
XLA Ops:
  12.1 2.1 fusion
  14.2 1.2 fusion.125
  15.4 86.2 %all-gather.2.cloned.1.call-done = bf16[2048,1792]{1,0:T(8,128)(2,1)} async-done(((bf16[16,1792]{1,0:T(8,128)(2,1)}), bf16[2048,1792]{1,0:T(8,128)(2,1)}) %all-gather.2.cloned.1.call-update) | async-done | bytes 7340048 | tf_op jit(solution)/shard_map/all_gather | solution.py:26
  101.6 3.7 %fusion.56 = f32[512,512]{1,0:T(8,128)S(1)} fusion(bf16[2048,1792]{1,0:T(8,128)(2,1)} %all-gather.2.cloned.1.call-done, bf16[512,2048]{1,0:T(8,128)(2,1)} %param.12, f32[2048]{0:T(1024)S(1)} %convert_element_type.78, f32[512]{0:T(512)S(1)} %add_rsqrt_fusion.1), kind=kOutput, calls=%fused_computation.38 | convolution fusion | flops 1079246848 | bytes 5253120 | tf_op jit(solution)/shard_map/dot_general | solution.py:117
  105.3 2.9 fusion.50
  108.2 2.1 collective-permute-start
  110.3 1.0 fusion.126
  111.3 3.3 %collective-permute-done = bf16[30,512]{1,0:T(8,128)(2,1)S(1)} collective-permute-done((bf16[30,512]{1,0:T(8,128)(2,1)S(1)}, bf16[30,512]{1,0:T(8,128)(2,1)S(1)}, u32[]{:S(2)}, u32[]{:S(2)}) %collective-permute-start) | collective-permute-done | bytes 30752 | tf_op jit(solution)/shard_map/ppermute | solution.py:33
  114.8 5.0 %fusion.123 = (f32[512]{0:T(512)S(1)}, f32[512]{0:T(512)S(1)}, f32[512,512]{1,0:T(8,128)S(1)}) fusion(f32[542,512]{1,0:T(8,128)S(1)} %maximum_convert_fusion, f32[512]{0:T(512)S(1)} %bitcast.147, f32[512]{0:T(512)S(1)} %bitcast.148, f32[512]{0:T(512)S(1)} %bitcast.119, f32[512]{0:T(512)S(1)} %bitcast.120, f32[512]{0:T(512)S(1)} %bitcast.121, ...), kind=kLoop, calls=%fused_computation.167 | loop fusion | flops 16776192 | bytes 33622016 | tf_op jit(solution)/shard_map/reduce_sum | solution.py:143
  120.5 4.3 %all-to-all-start = ((f32[4,1,1024]{2,1,0:T(1,128)}), f32[4,1,1024]{2,1,0:T(1,128)S(1)}, u32[]{:S(2)}, u32[]{:S(2)}) async-start(f32[4,1,1024]{2,1,0:T(1,128)} %broadcast_in_dim.14), calls=%async_computation | async-start | bytes 32768 | tf_op jit(solution)/shard_map/all_to_all | solution.py:38
  124.8 5.3 %all-to-all-done = f32[4,1,1024]{2,1,0:T(1,128)S(1)} async-done(((f32[4,1,1024]{2,1,0:T(1,128)}), f32[4,1,1024]{2,1,0:T(1,128)S(1)}, u32[]{:S(2)}, u32[]{:S(2)}) %all-to-all-start) | async-done | bytes 16416 | tf_op jit(solution)/shard_map/all_to_all | solution.py:38
  130.1 2.6 stack.2
  132.7 11.5 %all-to-all-start.1 = ((bf16[128,16,1024]{2,1,0:T(8,128)(2,1)}), bf16[128,16,1024]{2,1,0:T(8,128)(2,1)}, u32[]{:S(2)}, u32[]{:S(2)}) async-start(bf16[128,16,1024]{2,1,0:T(8,128)(2,1)} %stack.2), calls=%async_computation.1 | async-start | bytes 8388608 | tf_op jit(solution)/shard_map/all_to_all | solution.py:19
  145.3 0.9 broadcast_and_fusion
  146.1 1.9 convolution_convert_fusion
  148.8 2.2 collective-permute-start.2
  151.0 3.0 %fusion.47 = bf16[512,512]{0,1:T(8,128)(2,1)S(1)} fusion(bf16[2048,1792]{1,0:T(8,128)(2,1)} %all-gather.2.cloned.1.call-done, bf16[512,2048]{1,0:T(8,128)(2,1)S(1)} %copy-done, f32[2048]{0:T(1024)S(1)} %convert_element_type.78, f32[512]{0:T(512)S(1)} %add_rsqrt_fusion.1), kind=kOutput, calls=%fused_computation.35 | convolution fusion | flops 1078198272 | bytes 4728832 | tf_op jit(solution)/shard_map/dot_general | solution.py:117
  154.1 0.9 subtract_convert_fusion
  155.0 1.9 convolution_convert_fusion.1
  157.6 0.9 slice.310
  158.5 2.5 collective-permute-start.1
  161.0 1.0 concatenate.57
  162.2 72.4 %collective-permute-done.2 = bf16[128,2,64]{0,2,1:T(8,128)(2,1)} collective-permute-done((bf16[128,2,64]{0,2,1:T(8,128)(2,1)}, bf16[128,2,64]{0,2,1:T(8,128)(2,1)}, u32[]{:S(2)}, u32[]{:S(2)}) %collective-permute-start.2) | collective-permute-done | bytes 32800 | tf_op jit(solution)/shard_map/ppermute | solution.py:33
  234.6 0.8 copy_bitcast_fusion
  235.4 0.9 copy_bitcast_fusion.1
  236.3 2.0 fusion.4
  238.4 0.9 fusion.59
  239.8 6.6 %all-to-all-done.1 = bf16[128,16,1024]{2,1,0:T(8,128)(2,1)} async-done(((bf16[128,16,1024]{2,1,0:T(8,128)(2,1)}), bf16[128,16,1024]{2,1,0:T(8,128)(2,1)}, u32[]{:S(2)}, u32[]{:S(2)}) %all-to-all-start.1) | async-done | bytes 4194336 | tf_op jit(solution)/shard_map/all_to_all | solution.py:19
  246.4 3.0 %fusion.13 = f32[512,2048]{1,0:T(8,128)S(1)} fusion(bf16[2048,1024]{1,0:T(8,128)(2,1)} %bitcast.33, f32[512,512]{1,0:T(8,128)S(1)} %get-tuple-element.4, f32[512]{0:T(512)S(1)} %copy-done.10, f32[512]{0:T(512)S(1)} %get-tuple-element.41, f32[512]{0:T(512)S(1)} %get-tuple-element.40), kind=kOutput, calls=%fused_computation.17 | convolution fusion | flops 1075838976 | bytes 7346176 | tf_op jit(solution)/shard_map/dot_general | solution.py:184
  249.5 2.9 %add_convert_fusion = bf16[512,2048]{1,0:T(8,128)(2,1)S(1)} fusion(f32[512,2048]{1,0:T(8,128)S(1)} %fusion.13, bf16[2048,1024]{1,0:T(8,128)(2,1)} %bitcast.33, bf16[64,8,4,128]{3,2,1,0:T(4,128)(2,1)S(1)} %bitcast.110), kind=kOutput, calls=%fused_computation.12 | convolution fusion | flops 1075838976 | bytes 8912896 | tf_op jit(solution)/shard_map/dot_general | solution.py:185
  252.4 29.1 %all_to_all.16 = bf16[4,128,2048]{2,1,0:T(8,128)(2,1)S(1)} all-to-all(bf16[4,128,2048]{2,1,0:T(8,128)(2,1)S(1)} %bitcast.109), channel_id=1, replica_groups=mesh['sp'=128,'tp'=4] {'tp'}, dimensions={0} | all-to-all | bytes 4194304 | tf_op jit(solution)/shard_map/all_to_all | solution.py:76
  281.6 1.3 reduce_sum.62
  (62 shorter events, 9.0 us)
Async XLA Ops:
  7.2 94.4 %all-gather.2.cloned.1.call-start = ((), (), s32[]{:S(2)}) async-start(), calls=%async_computation.3 | async-start | bytes 7397376 | tf_op jit(solution)/shard_map/all_gather | solution.py:26
  10.8 0.6 copy-start.3
  12.1 138.9 %copy-start.7 = (f32[2048]{0:T(1024)}, f32[2048]{0:T(1024)S(1)}, u32[]{:S(2)}) copy-start(f32[2048]{0:T(1024)S(1)} %convert_element_type.78) | copy-start | bytes 24580
  14.2 136.8 %copy-start.8 = (f32[512]{0:T(512)}, f32[512]{0:T(512)S(1)}, u32[]{:S(2)}) copy-start(f32[512]{0:T(512)S(1)} %add_rsqrt_fusion.1) | copy-start | bytes 6148
  15.4 89.9 %copy-start = (bf16[512,2048]{1,0:T(8,128)(2,1)S(1)}, bf16[512,2048]{1,0:T(8,128)(2,1)}, u32[]{:S(2)}) copy-start(bf16[512,2048]{1,0:T(8,128)(2,1)} %param.12) | copy-start | bytes 6291460
  108.2 6.4 %collective-permute-start = (bf16[30,512]{1,0:T(8,128)(2,1)S(1)}, bf16[30,512]{1,0:T(8,128)(2,1)S(1)}, u32[]{:S(2)}, u32[]{:S(2)}) collective-permute-start(bf16[30,512]{1,0:T(8,128)(2,1)S(1)} %slice.319), channel_id=1, source_target_pairs={{0,4},{4,8},{8,12},{12,16},{16,20},{20,24},{24,28},{28,32},{32,36}... | collective-permute-start | bytes 92168 | tf_op jit(solution)/shard_map/ppermute | solution.py:33
  114.8 10.0 %copy-start.5 = (bf16[512,16]{0,1:T(8,128)(2,1)S(1)}, bf16[512,16]{0,1:T(8,128)(2,1)}, u32[]{:S(2)}) copy-start(bf16[512,16]{0,1:T(8,128)(2,1)} %param.23) | copy-start | bytes 49156
  114.8 9.9 %copy-start.6 = (bf16[512,16]{0,1:T(8,128)(2,1)S(1)}, bf16[512,16]{0,1:T(8,128)(2,1)}, u32[]{:S(2)}) copy-start(bf16[512,16]{0,1:T(8,128)(2,1)} %param.22) | copy-start | bytes 49156
  120.5 9.6 %all-to-all-start = ((f32[4,1,1024]{2,1,0:T(1,128)}), f32[4,1,1024]{2,1,0:T(1,128)S(1)}, u32[]{:S(2)}, u32[]{:S(2)}) async-start(f32[4,1,1024]{2,1,0:T(1,128)} %broadcast_in_dim.14), calls=%async_computation | async-start | bytes 32768 | tf_op jit(solution)/shard_map/all_to_all | solution.py:38
  132.7 11.5 %copy-start.11 = (f32[8]{0:T(128)S(1)}, f32[8]{0:T(128)}, u32[]{:S(2)}) copy-start(f32[8]{0:T(128)} %param.21) | copy-start | bytes 100
  132.7 113.8 %all-to-all-start.1 = ((bf16[128,16,1024]{2,1,0:T(8,128)(2,1)}), bf16[128,16,1024]{2,1,0:T(8,128)(2,1)}, u32[]{:S(2)}, u32[]{:S(2)}) async-start(bf16[128,16,1024]{2,1,0:T(8,128)(2,1)} %stack.2), calls=%async_computation.1 | async-start | bytes 8388608 | tf_op jit(solution)/shard_map/all_to_all | solution.py:19
  148.8 85.8 %collective-permute-start.2 = (bf16[128,2,64]{0,2,1:T(8,128)(2,1)}, bf16[128,2,64]{0,2,1:T(8,128)(2,1)}, u32[]{:S(2)}, u32[]{:S(2)}) collective-permute-start(bf16[128,2,64]{0,2,1:T(8,128)(2,1)} %pad_maximum_fusion.3), channel_id=1, source_target_pairs={{0,4},{4,8},{8,12},{12,16},{16,20},{20,24},{24,28},{28,32},{32,36}... | collective-permute-start | bytes 98312 | tf_op jit(solution)/shard_map/ppermute | solution.py:33
  156.9 0.7 copy-start.1
  158.5 76.9 %collective-permute-start.1 = (bf16[128,2,64]{0,2,1:T(8,128)(2,1)S(1)}, bf16[128,2,64]{0,2,1:T(8,128)(2,1)S(1)}, u32[]{:S(2)}, u32[]{:S(2)}) collective-permute-start(bf16[128,2,64]{0,2,1:T(8,128)(2,1)S(1)} %bitcast.114), channel_id=1, source_target_pairs={{0,4},{4,8},{8,12},{12,16},{16,20},{20,24},{24,28},{28,32},{32,36}... | collective-permute-start | bytes 98312 | tf_op jit(solution)/shard_map/ppermute | solution.py:33
  162.1 76.2 %copy-start.9 = (f32[2,4]{1,0:T(2,128)S(1)}, f32[2,4]{1,0:T(2,128)}, u32[]{:S(2)}) copy-start(f32[2,4]{1,0:T(2,128)} %add.243) | copy-start | bytes 100
  162.1 76.3 %copy-start.2 = (pred[4,128,256]{1,2,0:T(8,128)(4,1)S(1)}, pred[4,128,256]{1,2,0:T(8,128)(4,1)}, u32[]{:S(2)}) copy-start(pred[4,128,256]{1,2,0:T(8,128)(4,1)} %broadcast_and_fusion) | copy-start | bytes 393220
  238.3 8.1 %copy-start.10 = (f32[512]{0:T(512)S(1)}, f32[512]{0:T(512)}, u32[]{:S(2)}) copy-start(f32[512]{0:T(512)} %param.20) | copy-start | bytes 6148
  238.4 11.1 %copy-start.4 = (f32[4,2,4,128]{3,2,1,0:T(4,128)}, f32[4,2,4,128]{3,2,1,0:T(4,128)S(1)}, u32[]{:S(2)}) copy-start(f32[4,2,4,128]{3,2,1,0:T(4,128)S(1)} %add_log_fusion) | copy-start | bytes 49156
Sparse Core Ops, SparseCore 0:
  11.7 89.8 all-gather.1
